TPU v7x, 32 devices: a whole 2x2x4 slice. The times are simulated.
32 devices in a mesh: sp: 8 (over z, y), tp: 4 (over x, core).
Axes of the slice: x: 2, y: 2, z: 4, core: 2. Of those that a mesh axis runs over, the one named last changes fastest.
Arguments:
- q_proj: bfloat16 [4096, 1024], P('sp', 'tp'), may hold values from -5.25 to 5.25
- k_proj: bfloat16 [4096, 512], P('sp', 'tp'), may hold values from -5.25 to 5.25
- v_proj: bfloat16 [4096, 512], P('sp', 'tp'), may hold values from -6 to 6
- doc_ids: int32 [4096], P('sp'), may hold values from 0 to 3, never falling along the last dimension, each value on 1 to 2048 neighbouring positions
- sinks: float32 [16], P('tp'), may hold values from 0.5 to 5.5
- resid: bfloat16 [4096, 2048], P(('sp', 'tp')), may hold values from -12 to 12
- w_out: bfloat16 [1024, 2048], P('tp'), may hold values from -4 to 4
- norm_gain: float32 [2048], replicated, may hold values from 0.1 to 1.9
- w_gate: bfloat16 [2048, 5632], P('sp', 'tp'), may hold values from -0.125 to 0.125
- w_up: bfloat16 [2048, 5632], P('sp', 'tp'), may hold values from -0.125 to 0.125
- w_down: bfloat16 [5632, 2048], P('tp', 'sp'), may hold values from -0.078125 to 0.078125
Outputs:
- layer_out: bfloat16 [4096, 2048], P(('sp', 'tp'))
Inputs may be any that keep to these rules, and one draw needn't show every extreme that they name: `doc_ids`: document numbers never fall along the sequence; each document covers at most 2048 positions and one covers exactly that many.
All inputs are finite; a program needn't handle non-finite values.
Results may differ from a plain program's by a relative error of at most 0.015.
Values may be sent and summed in bfloat16 or wider, within the bound.
A program may use at most 64 MiB of HBM per device.

v0:
```python
import jax
import jax.numpy as jnp
from jax import lax
from jax.sharding import PartitionSpec as P

HEAD = 64
WINDOW = 128


norm_eps = 1e-06
masked = -1e30


def with_halo(block, sides, width):
    for axis, dim in sides:
        count = lax.axis_size(axis)
        forward = [(i, i + 1) for i in range(count - 1)]
        backward = [(target, source) for source, target in forward]
        low = lax.ppermute(
            lax.slice_in_dim(block, block.shape[dim] - width, None, axis=dim), axis, forward
        )
        high = lax.ppermute(lax.slice_in_dim(block, 0, width, axis=dim), axis, backward)
        block = jnp.concatenate([low, block, high], axis=dim)
    return block


def normalize(middle, norm_gain):
    return (
        middle * lax.rsqrt(jnp.mean(middle * middle, axis=-1, keepdims=True) + norm_eps) * norm_gain
    ).astype(jnp.bfloat16)


def band_view(extended, block_count):
    shaped = extended.reshape((block_count + 2, WINDOW) + extended.shape[1:])
    return jnp.concatenate([shaped[:-2], shaped[1:-1], shaped[2:]], axis=1)


def shards(q_proj, k_proj, v_proj, doc_ids, sinks, resid, w_out, norm_gain, w_gate, w_up, w_down):
    tok_rows = q_proj.shape[0]
    kv_local = k_proj.shape[1] // HEAD
    groups = q_proj.shape[1] // HEAD // kv_local
    block_count = tok_rows // WINDOW
    full_out = lax.all_gather(w_out, "tp", axis=0, tiled=True)
    keys_ext, values_ext, docs_ext = (
        with_halo(k_proj, (("sp", 0),), WINDOW),
        with_halo(v_proj, (("sp", 0),), WINDOW),
        with_halo(doc_ids, (("sp", 0),), WINDOW),
    )
    positions = (
        lax.axis_index("sp") * tok_rows
        - WINDOW
        + jnp.arange(tok_rows + 2 * WINDOW, dtype=jnp.int32)
    )
    inside = (positions >= 0) & (positions < tok_rows * lax.axis_size("sp"))
    docs_ext = jnp.where(inside, docs_ext, -1)
    key_band = band_view(keys_ext.reshape(tok_rows + 2 * WINDOW, kv_local, HEAD), block_count)
    value_band = band_view(values_ext.reshape(tok_rows + 2 * WINDOW, kv_local, HEAD), block_count)
    doc_band = band_view(docs_ext, block_count)
    queries = q_proj.reshape(block_count, WINDOW, kv_local, groups, HEAD)
    scores = jnp.einsum(
        "bqhgd,bkhd->bhgqk", queries, key_band, preferred_element_type=jnp.float32
    ) * HEAD ** (-0.5)
    offsets = jnp.arange(3 * WINDOW, dtype=jnp.int32) - WINDOW
    near = jnp.abs(jnp.arange(WINDOW, dtype=jnp.int32)[:, None] - offsets[None, :]) <= WINDOW
    query_docs = doc_ids.reshape(block_count, WINDOW)
    valid = near[None] & (query_docs[:, :, None] == doc_band[:, None, :])
    scores = jnp.where(valid[:, None, None], scores, masked)
    sink_table = sinks.reshape(kv_local, groups)[None, :, :, None, None]
    top = jnp.maximum(jnp.max(scores, axis=-1, keepdims=True), sink_table)
    expd = jnp.exp(scores - top)
    probs = (expd / (jnp.sum(expd, axis=-1, keepdims=True) + jnp.exp(sink_table - top))).astype(
        jnp.bfloat16
    )
    attended = jnp.einsum(
        "bhgqk,bkhd->bqhgd", probs, value_band, preferred_element_type=jnp.float32
    )
    attended = attended.astype(jnp.bfloat16).reshape(tok_rows, kv_local * groups * HEAD)
    own_rows = lax.all_to_all(attended, "tp", split_axis=0, concat_axis=1, tiled=True)
    projected = jnp.dot(own_rows, full_out, preferred_element_type=jnp.float32)
    middle = resid.astype(jnp.float32) + projected
    normed = lax.all_gather(normalize(middle, norm_gain), "tp", axis=0, tiled=True)

    def add_rows(piece):
        return jnp.dot(normed, piece, preferred_element_type=jnp.float32)

    gate = add_rows(lax.all_gather(w_gate, "sp", axis=0, tiled=True))
    up_part = add_rows(lax.all_gather(w_up, "sp", axis=0, tiled=True))
    hidden = (jax.nn.silu(gate) * up_part).astype(jnp.bfloat16)
    down_full = lax.all_gather(w_down, "sp", axis=1, tiled=True)
    summed_down = lax.psum_scatter(
        jnp.dot(hidden, down_full, preferred_element_type=jnp.float32).astype(jnp.bfloat16),
        "tp",
        scatter_dimension=0,
        tiled=True,
    ).astype(jnp.float32)
    return (middle + summed_down).astype(jnp.bfloat16)


def solution(mesh):
    placed = (
        P("sp", "tp"),
        P("sp", "tp"),
        P("sp", "tp"),
        P("sp"),
        P("tp"),
        P(("sp", "tp"), None),
        P("tp", None),
        P(),
        P("sp", "tp"),
        P("sp", "tp"),
        P("tp", "sp"),
    )
    return jax.shard_map(
        shards, mesh=mesh, in_specs=placed, out_specs=P(("sp", "tp"), None), check_vma=False
    )
```

profile of v0, /device:TPU:0, one launch (start us, length us, event | category | flops | bytes accessed | tf_op | source)
XLA Modules:
  0.0 408.3 jit_solution(3084332801912330174)
XLA Ops:
  6.5 0.0 all-gather.6.cloned.1.call-start
  6.6 0.7 all-gather.6.cloned.1.call-update
  7.3 0.0 all-gather.8.cloned.1.call-start
  7.3 0.8 fusion.27
  8.1 4.9 %collective-permute-start.2 = (s32[128]{0:T(128)S(1)}, s32[128]{0:T(128)S(1)}, u32[]{:S(2)}, u32[]{:S(2)}) collective-permute-start(s32[128]{0:T(128)S(1)} %get-tuple-element.16), channel_id=1, source_target_pairs={{0,4},{4,8},{8,12},{12,16},{16,20},{20,24},{24,28},{1,5},{5,9},{9,... | collective-permute-start | bytes 1544 | tf_op jit(solution)/shard_map/ppermute | solution.py:19
  13.0 1.3 collective-permute-start.3
  14.3 0.8 fusion.25
  15.1 4.5 %collective-permute-start.4 = (bf16[128,128]{1,0:T(8,128)(2,1)S(1)}, bf16[128,128]{1,0:T(8,128)(2,1)S(1)}, u32[]{:S(2)}, u32[]{:S(2)}) collective-permute-start(bf16[128,128]{1,0:T(8,128)(2,1)S(1)} %get-tuple-element.11), channel_id=1, source_target_pairs={{0,4},{4,8},{8,12},{12,16},{16,20},{20,24},{24,28},{1,5},{5,9},{9,... | collective-permute-start | bytes 98312 | tf_op jit(solution)/shard_map/ppermute | solution.py:19
  19.6 1.3 collective-permute-start.5
  20.9 0.8 fusion.24
  21.7 4.9 %collective-permute-start = (bf16[128,128]{1,0:T(8,128)(2,1)S(1)}, bf16[128,128]{1,0:T(8,128)(2,1)S(1)}, u32[]{:S(2)}, u32[]{:S(2)}) collective-permute-start(bf16[128,128]{1,0:T(8,128)(2,1)S(1)} %get-tuple-element.7), channel_id=1, source_target_pairs={{0,4},{4,8},{8,12},{12,16},{16,20},{20,24},{24,28},{1,5},{5,9},{9,... | collective-permute-start | bytes 98312 | tf_op jit(solution)/shard_map/ppermute | solution.py:19
  26.6 1.0 reshape.90
  27.7 1.0 reshape.87
  28.8 0.1 abs_compare_fusion
  28.9 1.2 reshape.92
  30.1 0.1 copy.24
  30.3 0.0 copy-done.6
  30.3 0.1 max.18
  30.4 0.1 copy.18
  30.5 0.0 collective-permute-done.2
  30.5 1.3 collective-permute-start.1
  31.8 0.0 collective-permute-done.3
  31.8 0.0 copy-done.3
  31.9 0.3 compare_and_fusion
  32.2 0.0 collective-permute-done.4
  32.2 0.0 collective-permute-done.5
  32.2 0.1 reshape.89
  32.4 0.1 copy.23
  32.5 0.1 reshape.91
  32.7 0.1 copy.25
  32.8 0.0 collective-permute-done
  32.8 4.4 %collective-permute-done.1 = bf16[128,128]{1,0:T(8,128)(2,1)S(1)} collective-permute-done((bf16[128,128]{1,0:T(8,128)(2,1)S(1)}, bf16[128,128]{1,0:T(8,128)(2,1)S(1)}, u32[]{:S(2)}, u32[]{:S(2)}) %collective-permute-start.1) | collective-permute-done | bytes 32800 | tf_op jit(solution)/shard_map/ppermute | solution.py:22
  37.3 0.1 reshape.86
  37.4 0.1 copy.17
  37.5 0.1 reshape.88
  37.7 0.1 copy.19
  37.8 0.7 fusion.2
  38.5 0.1 broadcast_maximum_fusion
  38.6 0.7 fusion.1
  39.3 0.1 exponential_add_fusion
  39.4 0.0 copy-start.2
  39.4 1.0 fusion.4
  40.4 8.6 %all_to_all.19 = bf16[4,128,256]{1,2,0:T(8,128)(2,1)S(1)} all-to-all(bf16[4,128,256]{1,2,0:T(8,128)(2,1)S(1)} %bitcast.42), channel_id=1, replica_groups=mesh['sp'=8,'tp'=4] {'tp'}, dimensions={0} | all-to-all | bytes 524288 | tf_op jit(solution)/shard_map/all_to_all | solution.py:78
  48.9 0.0 copy-done.2
  49.0 3.0 multiply_reduce_fusion
  52.0 0.0 copy-done.4
  52.0 1.0 multiply_convert_fusion
  52.9 0.0 all-gather.8.cloned.1.call-update
  53.0 0.0 all-gather.10.cloned.1.call-start
  53.0 0.7 all-gather.10.cloned.1.call-update
  53.7 0.0 all-gather.12.cloned.1.call-start
  53.7 0.5 all-gather.12.cloned.1.call-update
  54.3 0.0 all-gather.14.cloned.1.call-start
  54.3 0.5 all-gather.14.cloned.1.call-update
  54.9 0.2 reduce-scatter.2.cloned.1.call-start
  55.1 21.3 %all-gather.8.cloned.1.call-done = bf16[512,2048]{1,0:T(8,128)(2,1)} async-done(((bf16[128,2048]{1,0:T(8,128)(2,1)}), bf16[512,2048]{1,0:T(8,128)(2,1)}) %all-gather.8.cloned.1.call-update) | async-done | bytes 2097168 | tf_op jit(solution)/shard_map/all_gather | solution.py:81
  76.4 94.5 %all-gather.10.cloned.1.call-done = bf16[2048,1408]{1,0:T(8,128)(2,1)} async-done(((bf16[256,1408]{1,0:T(8,128)(2,1)}), bf16[2048,1408]{1,0:T(8,128)(2,1)}) %all-gather.10.cloned.1.call-update) | async-done | bytes 5767184 | tf_op jit(solution)/shard_map/all_gather | solution.py:86
  170.9 8.3 %fusion.28 = f32[512,1408]{1,0:T(8,128)} fusion(bf16[512,2048]{1,0:T(8,128)(2,1)} %all-gather.8.cloned.1.call-done, bf16[2048,1408]{1,0:T(8,128)(2,1)} %all-gather.10.cloned.1.call-done), kind=kOutput, calls=%fused_computation.52 | convolution fusion | flops 2952790016 | bytes 10747904 | tf_op jit(solution)/shard_map/dot_general | solution.py:84
  179.2 84.3 %all-gather.12.cloned.1.call-done = bf16[2048,1408]{1,0:T(8,128)(2,1)} async-done(((bf16[256,1408]{1,0:T(8,128)(2,1)}), bf16[2048,1408]{1,0:T(8,128)(2,1)}) %all-gather.12.cloned.1.call-update) | async-done | bytes 5767184 | tf_op jit(solution)/shard_map/all_gather | solution.py:87
  263.5 93.2 %all-gather.14.cloned.1.call-done = bf16[1408,2048]{1,0:T(8,128)(2,1)} async-done(((bf16[1408,256]{1,0:T(8,128)(2,1)}), bf16[1408,2048]{1,0:T(8,128)(2,1)}) %all-gather.14.cloned.1.call-update) | async-done | bytes 5767184 | tf_op jit(solution)/shard_map/all_gather | solution.py:89
  356.7 13.3 %convolution_convert_fusion = bf16[512,2048]{1,0:T(8,128)(2,1)} fusion(bf16[1408,2048]{1,0:T(8,128)(2,1)} %all-gather.14.cloned.1.call-done, bf16[512,2048]{1,0:T(8,128)(2,1)S(1)} %copy-done.5, bf16[2048,1408]{1,0:T(8,128)(2,1)} %all-gather.12.cloned.1.call-done, f32[512,1408]{1,0:T(8,128)} %fusion.28), kind=kOutput, calls=%fused_computation.5 | convolution fusion | flops 5910953984 | bytes 18612224 | tf_op jit(solution)/shard_map/dot_general | solution.py:91
  370.0 0.0 reduce-scatter.2.cloned.1.call-update
  370.0 29.5 %reduce-scatter.2.cloned.1.call-done = bf16[128,2048]{1,0:T(8,128)(2,1)} async-done(((bf16[512,2048]{1,0:T(8,128)(2,1)}), bf16[128,2048]{1,0:T(8,128)(2,1)}) %reduce-scatter.2.cloned.1.call-update) | async-done | bytes 524304 | tf_op jit(solution)/shard_map/reduce_scatter | solution.py:90
  399.5 1.9 add_convert_fusion
  (17 shorter events, 0.1 us)
Async XLA Ops:
  6.5 25.3 %copy-start.3 = (s32[512]{0:T(512)S(1)}, s32[512]{0:T(512)}, u32[]{:S(2)}) copy-start(s32[512]{0:T(512)} %param.14) | copy-start | bytes 6148
  6.5 25.6 %copy-start = (bf16[512,128]{1,0:T(8,128)(2,1)S(1)}, bf16[512,128]{1,0:T(8,128)(2,1)}, u32[]{:S(2)}) copy-start(bf16[512,128]{1,0:T(8,128)(2,1)} %param.12) | copy-start | bytes 393220
  6.5 30.7 %copy-start.1 = (bf16[512,128]{1,0:T(8,128)(2,1)S(1)}, bf16[512,128]{1,0:T(8,128)(2,1)}, u32[]{:S(2)}) copy-start(bf16[512,128]{1,0:T(8,128)(2,1)} %param.13) | copy-start | bytes 393220
  6.5 23.7 %copy-start.6 = (f32[4]{0:T(128)S(1)}, f32[4]{0:T(128)}, u32[]{:S(2)}) copy-start(f32[4]{0:T(128)} %param.15) | copy-start | bytes 52
  6.5 42.4 %all-gather.6.cloned.1.call-start = ((), (), s32[]{:S(2)}) async-start(), calls=%async_computation.2 | async-start | bytes 5242880 | tf_op jit(solution)/shard_map/all_gather | solution.py:43
  7.3 69.1 %all-gather.8.cloned.1.call-start = ((), (), s32[]{:S(2)}) async-start(), calls=%async_computation.3 | async-start | bytes 2621440 | tf_op jit(solution)/shard_map/all_gather | solution.py:81
  8.1 22.4 %collective-permute-start.2 = (s32[128]{0:T(128)S(1)}, s32[128]{0:T(128)S(1)}, u32[]{:S(2)}, u32[]{:S(2)}) collective-permute-start(s32[128]{0:T(128)S(1)} %get-tuple-element.16), channel_id=1, source_target_pairs={{0,4},{4,8},{8,12},{12,16},{16,20},{20,24},{24,28},{1,5},{5,9},{9,... | collective-permute-start | bytes 1544 | tf_op jit(solution)/shard_map/ppermute | solution.py:19
  13.0 18.8 %collective-permute-start.3 = (s32[128]{0:T(128)S(1)}, s32[128]{0:T(128)S(1)}, u32[]{:S(2)}, u32[]{:S(2)}) collective-permute-start(s32[128]{0:T(128)S(1)} %get-tuple-element.17), channel_id=1, source_target_pairs={{4,0},{8,4},{12,8},{16,12},{20,16},{24,20},{28,24},{5,1},{9,5},{13... | collective-permute-start | bytes 1544 | tf_op jit(solution)/shard_map/ppermute | solution.py:22
  15.1 17.1 %collective-permute-start.4 = (bf16[128,128]{1,0:T(8,128)(2,1)S(1)}, bf16[128,128]{1,0:T(8,128)(2,1)S(1)}, u32[]{:S(2)}, u32[]{:S(2)}) collective-permute-start(bf16[128,128]{1,0:T(8,128)(2,1)S(1)} %get-tuple-element.11), channel_id=1, source_target_pairs={{0,4},{4,8},{8,12},{12,16},{16,20},{20,24},{24,28},{1,5},{5,9},{9,... | collective-permute-start | bytes 98312 | tf_op jit(solution)/shard_map/ppermute | solution.py:19
  19.6 12.6 %collective-permute-start.5 = (bf16[128,128]{1,0:T(8,128)(2,1)S(1)}, bf16[128,128]{1,0:T(8,128)(2,1)S(1)}, u32[]{:S(2)}, u32[]{:S(2)}) collective-permute-start(bf16[128,128]{1,0:T(8,128)(2,1)S(1)} %get-tuple-element.12), channel_id=1, source_target_pairs={{4,0},{8,4},{12,8},{16,12},{20,16},{24,20},{28,24},{5,1},{9,5},{13... | collective-permute-start | bytes 98312 | tf_op jit(solution)/shard_map/ppermute | solution.py:22
  21.7 11.1 %collective-permute-start = (bf16[128,128]{1,0:T(8,128)(2,1)S(1)}, bf16[128,128]{1,0:T(8,128)(2,1)S(1)}, u32[]{:S(2)}, u32[]{:S(2)}) collective-permute-start(bf16[128,128]{1,0:T(8,128)(2,1)S(1)} %get-tuple-element.7), channel_id=1, source_target_pairs={{0,4},{4,8},{8,12},{12,16},{16,20},{20,24},{24,28},{1,5},{5,9},{9,... | collective-permute-start | bytes 98312 | tf_op jit(solution)/shard_map/ppermute | solution.py:19
  30.5 6.7 %collective-permute-start.1 = (bf16[128,128]{1,0:T(8,128)(2,1)S(1)}, bf16[128,128]{1,0:T(8,128)(2,1)S(1)}, u32[]{:S(2)}, u32[]{:S(2)}) collective-permute-start(bf16[128,128]{1,0:T(8,128)(2,1)S(1)} %get-tuple-element.8), channel_id=1, source_target_pairs={{4,0},{8,4},{12,8},{16,12},{20,16},{24,20},{28,24},{5,1},{9,5},{13... | collective-permute-start | bytes 98312 | tf_op jit(solution)/shard_map/ppermute | solution.py:22
  39.4 9.6 %copy-start.2 = (bf16[128,2048]{1,0:T(8,128)(2,1)S(1)}, bf16[128,2048]{1,0:T(8,128)(2,1)}, u32[]{:S(2)}) copy-start(bf16[128,2048]{1,0:T(8,128)(2,1)} %param.16) | copy-start | bytes 1572868
  48.9 3.0 copy-start.4
  53.0 117.9 %all-gather.10.cloned.1.call-start = ((), (), s32[]{:S(2)}) async-start(), calls=%async_computation.4 | async-start | bytes 6488064 | tf_op jit(solution)/shard_map/all_gather | solution.py:86
  53.7 209.8 %all-gather.12.cloned.1.call-start = ((), (), s32[]{:S(2)}) async-start(), calls=%async_computation.5 | async-start | bytes 6488064 | tf_op jit(solution)/shard_map/all_gather | solution.py:87
  54.3 302.4 %all-gather.14.cloned.1.call-start = ((), (), s32[]{:S(2)}) async-start(), calls=%async_computation.6 | async-start | bytes 6488064 | tf_op jit(solution)/shard_map/all_gather | solution.py:89
  54.9 344.6 %reduce-scatter.2.cloned.1.call-start = ((), (), s32[]{:S(2)}) async-start(), calls=%async_computation.7 | async-start | bytes 2621440 | tf_op jit(solution)/shard_map/reduce_scatter | solution.py:90
  76.4 280.3 %copy-start.5 = (bf16[512,2048]{1,0:T(8,128)(2,1)S(1)}, bf16[512,2048]{1,0:T(8,128)(2,1)}, u32[]{:S(2)}) copy-start(bf16[512,2048]{1,0:T(8,128)(2,1)} %all-gather.8.cloned.1.call-done) | copy-start | bytes 6291460
Sparse Core Ops, SparseCore 0:
  8.9 37.1 all-gather.5
  53.1 23.2 all-gather.7
  78.5 92.3 all-gather.9
  172.9 90.4 all-gather.11
  265.3 91.2 all-gather.13
  370.1 29.3 reduce-scatter.1
where the time goes:
time: 409 us; the launch traced here: 408 us
  waiting for transfers between devices  330 us (81%)
  matrix products  26.2 us (6%)
  starting transfers between devices  18.6 us (5%)
  between operations  13.8 us (3%)
  blocking collectives  8.59 us (2%)
  local copies, waits for them, and re-layouts  7.14 us (2%)
  other arithmetic  4.2 us (1%)
    all_gather x1, waiting for transfers between devices, shards(): gate = add_rows(lax.all_gather(w_gate, 'sp', axis=0, tiled=True))  94.5 us
    all_gather x1, waiting for transfers between devices, shards(): down_full = lax.all_gather(w_down, 'sp', axis=1, tiled=True)  93.2 us
    all_gather x1, waiting for transfers between devices, shards(): up_part = add_rows(lax.all_gather(w_up, 'sp', axis=0, tiled=True))  84.3 us
    reduce_scatter x1, waiting for transfers between devices, shards(): lax.psum_scatter(jnp.dot(hidden, down_full, preferred_element_type=jnp.fl...  29.5 us
    all_gather x1, waiting for transfers between devices, shards(): lax.all_gather(normalize(middle, norm_gain), 'tp', axis=0, tiled=True)  21.3 us
    ppermute x3, starting transfers between devices, with_halo(): lax.ppermute(lax.slice_in_dim(block, block.shape[dim] - width, None, axis...  14.4 us
    dot_general x1, matrix products, shards(): jnp.dot(hidden, down_full, preferred_element_type=jnp.float32)  13.3 us
    all_to_all x1, blocking collectives, shards(): lax.all_to_all(attended, 'tp', split_axis=0, concat_axis=1, tiled=True)  8.59 us
  transfers between devices with their start and end apart: 12, of which 6 were waited for; matrix products, arithmetic and copies ran while one was open for 4% of the time, Pallas kernels for 0%

commit v1 on v0

v1 whole, which is shorter than its diff:
```python
import functools

import jax
import jax.numpy as jnp
from jax import lax
from jax.experimental import pallas as pl
from jax.experimental.pallas import tpu as pltpu
from jax.sharding import PartitionSpec as P

HEAD = 64
WINDOW = 128
norm_eps = 1e-06
masked = -1e30
MESH = pl.DeviceIdType.MESH


def kernel(
    Z, Y, T,
    q_ref, k_ref, v_ref, drow_ref, dcol_ref, sink_ref, resid_ref, gain_ref, wo_hbm, wg_hbm, wu_hbm, wd_hbm,
    out_ref,
    G, U, D, kext, vext, dext, att, rows, WO, mid, NB, gacc, uacc, hid, PT, RT,
    loc_sem, halo_s, halo_r, wo_s, wo_r, at_s, at_r, nb_s, nb_r, pt_s, pt_r, w_s, w_r, b_s,
):
    n_sp = Z * Y
    s, t = lax.axis_index("sp"), lax.axis_index("tp")
    z, y = s // Y, s % Y
    tok = q_ref.shape[0]
    nb = tok // WINDOW
    own = tok // T
    heads = q_ref.shape[1] // HEAD
    groups = heads // (k_ref.shape[1] // HEAD)
    kb = G.shape[1]
    ff = G.shape[2]
    half = D.shape[1] // 2
    mats = (G, U, D.at[:, half:], D.at[:, :half])

    def rcopy(src, dst, ssem, rsem, sp_to, tp_to):
        return pltpu.make_async_remote_copy(
            src_ref=src, dst_ref=dst, send_sem=ssem, recv_sem=rsem,
            device_id={"sp": sp_to, "tp": tp_to}, device_id_type=MESH,
        )

    def arrived(ref, sem):
        pltpu.make_async_copy(ref, ref, sem).wait()

    def piece(m, slot):
        if m < 2:
            return (G, U)[m].at[slot]
        return D.at[slot, pl.ds(half if m == 2 else 0, half)]

    locals_ = [
        pltpu.make_async_copy(wd_hbm, D.at[s], loc_sem.at[2]),
        pltpu.make_async_copy(wg_hbm, G.at[s], loc_sem.at[0]),
        pltpu.make_async_copy(wu_hbm, U.at[s], loc_sem.at[1]),
        pltpu.make_async_copy(wo_hbm, WO.at[t], loc_sem.at[3]),
    ]
    for c in locals_:
        c.start()

    right, left = (s + 1) % n_sp, (s + n_sp - 1) % n_sp
    halos = []
    for i, (src, dst) in enumerate(((k_ref, kext), (v_ref, vext))):
        halos.append((src.at[pl.ds(tok - WINDOW, WINDOW)], dst.at[pl.ds(0, WINDOW)], 2 * i, right))
        halos.append((src.at[pl.ds(0, WINDOW)], dst.at[pl.ds(tok + WINDOW, WINDOW)], 2 * i + 1, left))
    halos.append((drow_ref.at[nb - 1], dext.at[0], 4, right))
    halos.append((drow_ref.at[0], dext.at[nb + 1], 5, left))
    halo_copies = [rcopy(a, b, halo_s.at[i], halo_r.at[i], to, t) for a, b, i, to in halos]
    for c in halo_copies:
        c.start()

    def up_copy(m, slot, sem):
        return rcopy(piece(m, slot), piece(m, slot), sem, w_r.at[m, slot], s + Y, t)

    def down_copy(m, slot, sem):
        return rcopy(piece(m, slot), piece(m, slot), sem, w_r.at[m, slot], s - Y, t)

    def z_sem(m, way, zz, yy):
        return b_s.at[way, zz * Y + yy] if m == 3 else w_s.at[m, way, zz]

    def send_up(m, zz, yy):
        @pl.when(z + 1 < Z)
        def _():
            up_copy(m, zz * Y + yy, z_sem(m, 0, zz, yy)).start()

    def send_down(m, zz, yy):
        @pl.when(z > 0)
        def _():
            down_copy(m, zz * Y + yy, z_sem(m, 1, zz, yy)).start()

    def y_copies(m, zz):
        slot = zz * Y + y
        return [
            rcopy(piece(m, slot), piece(m, slot), w_s.at[m, 1 + j, zz], w_r.at[m, slot], z * Y + (y + j) % Y, t)
            for j in range(1, Y)
        ]

    def send_y(m, zz):
        for c in y_copies(m, zz):
            c.start()

    def tp_peers():
        return [(t + j) % T for j in range(1, T)]

    for c in locals_[:1]:
        c.wait()
    send_y(3, z)
    for m in (0, 1):
        locals_[1 + m].wait()
        send_up(m, z, y)
        send_down(m, z, y)
        send_y(m, z)
    locals_[3].wait()
    wo_copies = [rcopy(WO.at[t], WO.at[t], wo_s.at[j], wo_r.at[t], s, p) for j, p in enumerate(tp_peers())]
    for c in wo_copies:
        c.start()

    kext[pl.ds(WINDOW, tok)] = k_ref[...]
    vext[pl.ds(WINDOW, tok)] = v_ref[...]
    dext[pl.ds(1, nb)] = drow_ref[...]
    for a, b, i, to in halos:
        arrived(b, halo_r.at[i])
    row_at = lax.broadcasted_iota(jnp.int32, (WINDOW, 3 * WINDOW), 0)
    col_at = lax.broadcasted_iota(jnp.int32, (WINDOW, 3 * WINDOW), 1) - WINDOW
    near = jnp.abs(row_at - col_at) <= WINDOW

    @pl.loop(0, nb)
    def _(blk):
        base = pl.multiple_of(blk * WINDOW, WINDOW)
        place = s * tok + base + col_at
        key_docs = jnp.concatenate([dext[blk + i][0:1] for i in range(3)], axis=1)
        query_docs = dcol_ref[pl.ds(base, WINDOW), 0:1]
        valid = near & (place >= 0) & (place < tok * n_sp) & (query_docs == key_docs)
        qs = q_ref[pl.ds(base, WINDOW)]
        ks = kext[pl.ds(base, 3 * WINDOW)]
        vs = vext[pl.ds(base, 3 * WINDOW)]
        outs = []
        for h in range(heads):
            g = h // groups
            scores = lax.dot_general(
                qs[:, h * HEAD:(h + 1) * HEAD], ks[:, g * HEAD:(g + 1) * HEAD],
                (((1,), (1,)), ((), ())), preferred_element_type=jnp.float32,
            ) * HEAD ** (-0.5)
            scores = jnp.where(valid, scores, masked)
            sink = sink_ref[h]
            top = jnp.maximum(jnp.max(scores, axis=-1, keepdims=True), sink)
            expd = jnp.exp(scores - top)
            total = jnp.sum(expd, axis=-1, keepdims=True) + jnp.exp(sink - top)
            probs = (expd / total).astype(jnp.bfloat16)
            outs.append(jnp.dot(probs, vs[:, g * HEAD:(g + 1) * HEAD], preferred_element_type=jnp.float32))
        att[pl.ds(base, WINDOW)] = jnp.concatenate(outs, axis=1).astype(jnp.bfloat16)

    at_copies = [
        rcopy(att.at[pl.ds(pl.multiple_of(p * own, own), own)], rows.at[t], at_s.at[j], at_r.at[t], s, p)
        for j, p in enumerate(tp_peers())
    ]
    for c in at_copies:
        c.start()
    rows[t] = att[pl.ds(pl.multiple_of(t * own, own), own)]

    def handle(ms, r):
        for m in ms:
            for sign in (-1, 1):
                zz = z + sign * r

                @pl.when((zz >= 0) & (zz < Z))
                def _():
                    send = send_up if sign < 0 else send_down
                    columns = range(Y) if m == 3 else (0,)
                    for j in columns:
                        yy = (y + j) % Y
                        arrived(piece(m, zz * Y + yy), w_r.at[m, zz * Y + yy])
                        send(m, zz, yy)
                    if m != 3:
                        send_y(m, zz)

    def project():
        for p in tp_peers():
            arrived(WO.at[p], wo_r.at[p])
            arrived(rows.at[p], at_r.at[p])
        middle = resid_ref[...].astype(jnp.float32)
        for i in range(T):
            middle = middle + jnp.dot(rows[i], WO[i], preferred_element_type=jnp.float32)
        mid[...] = middle
        normed = (
            middle * lax.rsqrt(jnp.mean(middle * middle, axis=-1, keepdims=True) + norm_eps) * gain_ref[...]
        ).astype(jnp.bfloat16)
        mine = pl.ds(pl.multiple_of(t * own, own), own)
        for i in range(n_sp):
            NB[i, mine] = normed[:, i * kb:(i + 1) * kb]
        for c in nb_copies():
            c.start()

    def nb_rows(p):
        return NB.at[:, pl.ds(pl.multiple_of(p * own, own), own)]

    def nb_copies():
        return [rcopy(nb_rows(t), nb_rows(t), nb_s.at[j], nb_r.at[t], s, p) for j, p in enumerate(tp_peers())]

    step = min(tok, 256)

    def each(r, body):
        @pl.loop(0, (2 if r else 1) * Y)
        def _(i):
            joff = i % Y
            zz = z + (2 * (i // Y) - 1) * r
            slot = zz * Y + (y + joff) % Y

            @pl.when((zz >= 0) & (zz < Z))
            def _():
                body(slot, joff)

    def gate_up(r):
        def body(slot, joff):
            @pl.when(joff > 0)
            def _():
                for m in (0, 1):
                    arrived(piece(m, slot), w_r.at[m, slot])

            @pl.loop(0, tok // step)
            def _(i):
                at = pl.ds(pl.multiple_of(i * step, step), step)
                x = NB[slot, at]
                gacc[at] += jnp.dot(x, G[slot], preferred_element_type=jnp.float32)
                uacc[at] += jnp.dot(x, U[slot], preferred_element_type=jnp.float32)

        each(r, body)

    def pt_rows(slot, p):
        return PT.at[slot, pl.ds(pl.multiple_of(p * own, own), own)]

    def down(r):
        def body(slot, joff):
            @pl.when(joff > 0)
            def _():
                arrived(piece(2, slot), w_r.at[2, slot])

            @pl.loop(0, tok // step)
            def _(i):
                at = pl.ds(pl.multiple_of(i * step, step), step)
                PT[slot, at] = jnp.dot(hid[at], D[slot], preferred_element_type=jnp.float32).astype(jnp.bfloat16)

            for j, p in enumerate(tp_peers()):
                rcopy(pt_rows(slot, p), RT.at[t, slot], pt_s.at[j], pt_r.at[t], s, p).start()

        each(r, body)

    gacc[...] = jnp.zeros_like(gacc)
    uacc[...] = jnp.zeros_like(uacc)
    if Z > 1:
        handle((0, 1), 1)
    project()
    if Z > 2:
        handle((0, 1), 2)
    for p in tp_peers():
        arrived(nb_rows(p), nb_r.at[p])
    gate_up(0)
    for r in range(3, Z):
        handle((0, 1), r)
        gate_up(r - 2)

    for j in range(1, Y):
        slot = z * Y + (y + j) % Y
        arrived(piece(3, slot), w_r.at[3, slot])
    send_up(2, z, y)
    send_down(2, z, y)
    send_y(2, z)
    for j in range(Y):
        send_up(3, z, (y + j) % Y)
        send_down(3, z, (y + j) % Y)
    for r in range(max(1, Z - 2), Z - 1):
        gate_up(r)
    if Z > 1:
        handle((2, 3), 1)
        gate_up(Z - 1)

    @pl.loop(0, tok // WINDOW)
    def _(i):
        at = pl.ds(pl.multiple_of(i * WINDOW, WINDOW), WINDOW)
        gate = gacc[at]
        hid[at] = (gate / (1.0 + jnp.exp(-gate)) * uacc[at]).astype(jnp.bfloat16)

    down(0)
    for r in range(1, Z):
        if r + 1 < Z:
            handle((2, 3), r + 1)
        down(r)

    for p in tp_peers():
        arrived(RT.at[p], pt_r.at[p])
    for i in range(n_sp):
        cols = slice(i * kb, (i + 1) * kb)
        total = mid[:, cols] + PT[i, pl.ds(pl.multiple_of(t * own, own), own)].astype(jnp.float32)
        for p in tp_peers():
            total = total + RT[p, i].astype(jnp.float32)
        out_ref[:, cols] = total.astype(jnp.bfloat16)

    for c in halo_copies + wo_copies + at_copies + nb_copies():
        c.wait_send()
    for j, p in enumerate(tp_peers()):
        arrived(PT.at[:, pl.ds(pl.multiple_of(p * own, own), own)], pt_s.at[j])
    for c in y_copies(3, z):
        c.wait_send()
    for zz in range(Z):
        for m in range(3):
            for c in y_copies(m, zz):
                c.wait_send()
        for m in range(4):
            for j in range(Y if m == 3 else 1):
                yy = (y + j) % Y

                @pl.when((zz <= z) & (z + 1 < Z))
                def _():
                    up_copy(m, zz * Y + yy, z_sem(m, 0, zz, yy)).wait_send()

                @pl.when((zz >= z) & (z > 0))
                def _():
                    down_copy(m, zz * Y + yy, z_sem(m, 1, zz, yy)).wait_send()


def shards(Z, Y, T, q, k, v, doc_ids, sinks, resid, w_out, gain, wg, wu, wd):
    n_sp = Z * Y
    tok, (kb, ff), d = q.shape[0], wg.shape, resid.shape[1]
    nb, own = tok // WINDOW, tok // T
    bf, f32 = jnp.bfloat16, jnp.float32
    drow = jnp.broadcast_to(doc_ids.reshape(nb, 1, WINDOW), (nb, 8, WINDOW))
    dcol = jnp.broadcast_to(doc_ids[:, None], (tok, 128))
    vmem, hbm = pl.BlockSpec(memory_space=pltpu.VMEM), pl.BlockSpec(memory_space=pl.ANY)
    dma = pltpu.SemaphoreType.DMA
    V = pltpu.VMEM
    return pl.pallas_call(
        functools.partial(kernel, Z, Y, T),
        out_shape=jax.ShapeDtypeStruct((own, d), bf),
        in_specs=[vmem] * 5 + [pl.BlockSpec(memory_space=pltpu.SMEM)] + [vmem] * 2 + [hbm] * 4,
        out_specs=vmem,
        scratch_shapes=[
            V((n_sp, kb, ff), bf), V((n_sp, kb, ff), bf), V((n_sp, ff, wd.shape[1]), bf),
            V((tok + 2 * WINDOW, k.shape[1]), bf), V((tok + 2 * WINDOW, k.shape[1]), bf),
            V((nb + 2, 8, WINDOW), jnp.int32),
            V((tok, q.shape[1]), bf), V((T, own, q.shape[1]), bf), V((T,) + w_out.shape, bf),
            V((own, d), f32), V((n_sp, tok, kb), bf), V((tok, ff), f32), V((tok, ff), f32), V((tok, ff), bf),
            V((n_sp, tok, kb), bf), V((T, n_sp, own, kb), bf),
            dma((4,)), dma((6,)), dma((6,)),
            dma((T,)), dma((T,)), dma((T,)), dma((T,)), dma((T,)), dma((T,)), dma((T,)), dma((T,)),
            dma((4, 1 + Y, Z)), dma((4, n_sp)), dma((2, n_sp)),
        ],
        compiler_params=pltpu.CompilerParams(has_side_effects=True, vmem_limit_bytes=60 * 1024 * 1024),
    )(q, k, v, drow, dcol, sinks, resid, gain.reshape(1, d), w_out, wg, wu, wd)


def solution(mesh):
    n_sp, T = mesh.shape["sp"], mesh.shape["tp"]
    Y = 2 if n_sp <= 8 else 4
    while n_sp % Y:
        Y //= 2
    placed = (
        P("sp", "tp"),
        P("sp", "tp"),
        P("sp", "tp"),
        P("sp"),
        P("tp"),
        P(("sp", "tp"), None),
        P("tp", None),
        P(),
        P("sp", "tp"),
        P("sp", "tp"),
        P("tp", "sp"),
    )
    return jax.shard_map(
        functools.partial(shards, n_sp // Y, Y, T), mesh=mesh, in_specs=placed,
        out_specs=P(("sp", "tp"), None), check_vma=False,
    )
```

time: 409 us -> 215 us (0.53)
  waiting for transfers between devices: 330 us -> 0 us
  Pallas kernels: 0 us -> 211 us
  matrix products: 26.2 us -> 0 us
  starting transfers between devices: 18.6 us -> 0 us
  between operations: 13.8 us -> 0.01 us
  blocking collectives: 8.59 us -> 0 us
  other arithmetic: 4.2 us -> 0 us
    all_gather x5 -> x0, waiting for transfers between devices: 293 us -> none  [the longest x1 94.5 us: shards(): gate = add_rows(lax.all_gather(w_gate, 'sp', axis=0, tiled=True))]
    pallas_call x0 -> x1, Pallas kernels: none -> 211 us  [shards(): pl.pallas_call(functools.partial(kernel, Z, Y, T), out_shape=jax.ShapeDty...]
    reduce_scatter x1 -> x0, waiting for transfers between devices: 29.5 us -> none  [shards(): lax.psum_scatter(jnp.dot(hidden, down_full, preferred_element_type=jnp.fl...]
    dot_general x5 -> x0, matrix products: 26.2 us -> none  [the longest x1 13.3 us: shards(): jnp.dot(hidden, down_full, preferred_element_type=jnp.float32)]
    ppermute x6 -> x0, starting transfers between devices: 18.2 us -> none  [the longest x3 14.4 us: with_halo(): lax.ppermute(lax.slice_in_dim(block, block.shape[dim] - width, None, axis...]
    all_to_all x1 -> x0, blocking collectives: 8.59 us -> none  [shards(): lax.all_to_all(attended, 'tp', split_axis=0, concat_axis=1, tiled=True)]
    slice x16 -> x0, local copies, waits for them, and re-layouts: 5.8 us -> none  [the longest x13 3.46 us: band_view(): return jnp.concatenate([shaped[:-2], shaped[1:-1], shaped[2:]], axis=1)]
    ppermute x6 -> x0, waiting for transfers between devices: 4.44 us -> none  [the longest x3 4.43 us: with_halo(): lax.ppermute(lax.slice_in_dim(block, 0, width, axis=dim), axis, backward)]
  transfers between devices with their start and end apart: 12 -> 0, of which waited for: 6 -> 0; matrix products, arithmetic and copies ran while one was open for 4% -> 0% of each run, Pallas kernels for 0% -> 0%
where the time goes in v1:
time: 215 us
  Pallas kernels  211 us (98%)
  local copies, waits for them, and re-layouts  4 us (2%)
    pallas_call x1, Pallas kernels, shards(): pl.pallas_call(functools.partial(kernel, Z, Y, T), out_shape=jax.ShapeDty...  211 us

profile of v1, /device:TPU:0, one launch (start us, length us, event | category | flops | bytes accessed | tf_op | source)
XLA Modules:
  0.0 215.1 jit_solution(1421015311748124706)
XLA Ops:
  0.0 0.0 copy-start
  0.0 0.7 copy-done
  0.7 0.6 broadcast_in_dim.14.drow_ref
  1.3 0.8 broadcast_in_dim.15.dcol_ref
  2.1 211.0 %shard_map.109 = bf16[128,2048]{1,0:T(8,128)(2,1)} custom-call(bf16[512,256]{1,0:T(8,128)(2,1)} %q_ref.1, bf16[512,128]{1,0:T(8,128)(2,1)} %k_ref.1, bf16[512,128]{1,0:T(8,128)(2,1)} %v_ref.1, s32[4,8,128]{2,1,0:T(8,128)} %broadcast_in_dim.14.drow_ref, s32[512,128]{1,0:T(8,128)} %broadcast_in_dim.15.dcol_ref, f32[4]{0:T(128)} %sink_ref.1, ...), custom_call_target="tpu_custom_call" | custom-call | tf_op jit(solution)/shard_map/pallas_call | solution.py:330
  213.2 1.9 copy.13
Async XLA Ops:
  0.0 0.7 copy-start

commit v2 on v1

--- a/solution.py
+++ b/solution.py
@@ -14,111 +14,15 @@
 MESH = pl.DeviceIdType.MESH
 
 
-def kernel(
-    Z, Y, T,
-    q_ref, k_ref, v_ref, drow_ref, dcol_ref, sink_ref, resid_ref, gain_ref, wo_hbm, wg_hbm, wu_hbm, wd_hbm,
-    out_ref,
-    G, U, D, kext, vext, dext, att, rows, WO, mid, NB, gacc, uacc, hid, PT, RT,
-    loc_sem, halo_s, halo_r, wo_s, wo_r, at_s, at_r, nb_s, nb_r, pt_s, pt_r, w_s, w_r, b_s,
-):
-    n_sp = Z * Y
-    s, t = lax.axis_index("sp"), lax.axis_index("tp")
-    z, y = s // Y, s % Y
+def attend(n_sp, s, q_ref, k_ref, v_ref, drow_ref, dcol_ref, sink_ref, kext, vext, dext, att, wait_halo):
     tok = q_ref.shape[0]
     nb = tok // WINDOW
-    own = tok // T
     heads = q_ref.shape[1] // HEAD
     groups = heads // (k_ref.shape[1] // HEAD)
-    kb = G.shape[1]
-    ff = G.shape[2]
-    half = D.shape[1] // 2
-    mats = (G, U, D.at[:, half:], D.at[:, :half])
-
-    def rcopy(src, dst, ssem, rsem, sp_to, tp_to):
-        return pltpu.make_async_remote_copy(
-            src_ref=src, dst_ref=dst, send_sem=ssem, recv_sem=rsem,
-            device_id={"sp": sp_to, "tp": tp_to}, device_id_type=MESH,
-        )
-
-    def arrived(ref, sem):
-        pltpu.make_async_copy(ref, ref, sem).wait()
-
-    def piece(m, slot):
-        if m < 2:
-            return (G, U)[m].at[slot]
-        return D.at[slot, pl.ds(half if m == 2 else 0, half)]
-
-    locals_ = [
-        pltpu.make_async_copy(wd_hbm, D.at[s], loc_sem.at[2]),
-        pltpu.make_async_copy(wg_hbm, G.at[s], loc_sem.at[0]),
-        pltpu.make_async_copy(wu_hbm, U.at[s], loc_sem.at[1]),
-        pltpu.make_async_copy(wo_hbm, WO.at[t], loc_sem.at[3]),
-    ]
-    for c in locals_:
-        c.start()
-
-    right, left = (s + 1) % n_sp, (s + n_sp - 1) % n_sp
-    halos = []
-    for i, (src, dst) in enumerate(((k_ref, kext), (v_ref, vext))):
-        halos.append((src.at[pl.ds(tok - WINDOW, WINDOW)], dst.at[pl.ds(0, WINDOW)], 2 * i, right))
-        halos.append((src.at[pl.ds(0, WINDOW)], dst.at[pl.ds(tok + WINDOW, WINDOW)], 2 * i + 1, left))
-    halos.append((drow_ref.at[nb - 1], dext.at[0], 4, right))
-    halos.append((drow_ref.at[0], dext.at[nb + 1], 5, left))
-    halo_copies = [rcopy(a, b, halo_s.at[i], halo_r.at[i], to, t) for a, b, i, to in halos]
-    for c in halo_copies:
-        c.start()
-
-    def up_copy(m, slot, sem):
-        return rcopy(piece(m, slot), piece(m, slot), sem, w_r.at[m, slot], s + Y, t)
-
-    def down_copy(m, slot, sem):
-        return rcopy(piece(m, slot), piece(m, slot), sem, w_r.at[m, slot], s - Y, t)
-
-    def z_sem(m, way, zz, yy):
-        return b_s.at[way, zz * Y + yy] if m == 3 else w_s.at[m, way, zz]
-
-    def send_up(m, zz, yy):
-        @pl.when(z + 1 < Z)
-        def _():
-            up_copy(m, zz * Y + yy, z_sem(m, 0, zz, yy)).start()
-
-    def send_down(m, zz, yy):
-        @pl.when(z > 0)
-        def _():
-            down_copy(m, zz * Y + yy, z_sem(m, 1, zz, yy)).start()
-
-    def y_copies(m, zz):
-        slot = zz * Y + y
-        return [
-            rcopy(piece(m, slot), piece(m, slot), w_s.at[m, 1 + j, zz], w_r.at[m, slot], z * Y + (y + j) % Y, t)
-            for j in range(1, Y)
-        ]
-
-    def send_y(m, zz):
-        for c in y_copies(m, zz):
-            c.start()
-
-    def tp_peers():
-        return [(t + j) % T for j in range(1, T)]
-
-    for c in locals_[:1]:
-        c.wait()
-    send_y(3, z)
-    for m in (0, 1):
-        locals_[1 + m].wait()
-        send_up(m, z, y)
-        send_down(m, z, y)
-        send_y(m, z)
-    locals_[3].wait()
-    wo_copies = [rcopy(WO.at[t], WO.at[t], wo_s.at[j], wo_r.at[t], s, p) for j, p in enumerate(tp_peers())]
-    for c in wo_copies:
-        c.start()
-
     kext[pl.ds(WINDOW, tok)] = k_ref[...]
     vext[pl.ds(WINDOW, tok)] = v_ref[...]
     dext[pl.ds(1, nb)] = drow_ref[...]
-    for a, b, i, to in halos:
-        arrived(b, halo_r.at[i])
+    wait_halo()
     row_at = lax.broadcasted_iota(jnp.int32, (WINDOW, 3 * WINDOW), 0)
     col_at = lax.broadcasted_iota(jnp.int32, (WINDOW, 3 * WINDOW), 1) - WINDOW
     near = jnp.abs(row_at - col_at) <= WINDOW
@@ -149,6 +53,108 @@
             outs.append(jnp.dot(probs, vs[:, g * HEAD:(g + 1) * HEAD], preferred_element_type=jnp.float32))
         att[pl.ds(base, WINDOW)] = jnp.concatenate(outs, axis=1).astype(jnp.bfloat16)
 
+
+def kernel(
+    Z, Y, T,
+    q_ref, k_ref, v_ref, drow_ref, dcol_ref, sink_ref, resid_ref, gain_ref, wo_hbm, wg_hbm, wu_hbm, wd_hbm,
+    out_ref,
+    G, U, D, kext, vext, dext, att, rows, WO, mid, NB, gacc, uacc, hid, PT, RT,
+    loc_sem, halo_s, halo_r, wo_s, wo_r, at_s, at_r, nb_s, nb_r, pt_s, pt_r, w_s, w_r, b_s,
+):
+    n_sp = Z * Y
+    s, t = lax.axis_index("sp"), lax.axis_index("tp")
+    z, y = s // Y, s % Y
+    tok = q_ref.shape[0]
+    nb = tok // WINDOW
+    own = tok // T
+    kb = G.shape[1]
+    half = D.shape[1] // 2
+
+    def rcopy(src, dst, ssem, rsem, sp_to, tp_to):
+        return pltpu.make_async_remote_copy(
+            src_ref=src, dst_ref=dst, send_sem=ssem, recv_sem=rsem,
+            device_id={"sp": sp_to, "tp": tp_to}, device_id_type=MESH,
+        )
+
+    def arrived(ref, sem):
+        pltpu.make_async_copy(ref, ref, sem).wait()
+
+    def piece(m, slot):
+        if m < 2:
+            return (G, U)[m].at[slot]
+        return D.at[slot, pl.ds(half if m == 2 else 0, half)]
+
+    locals_ = [
+        pltpu.make_async_copy(wd_hbm, D.at[s], loc_sem.at[2]),
+        pltpu.make_async_copy(wg_hbm, G.at[s], loc_sem.at[0]),
+        pltpu.make_async_copy(wu_hbm, U.at[s], loc_sem.at[1]),
+        pltpu.make_async_copy(wo_hbm, WO.at[t], loc_sem.at[3]),
+    ]
+    for c in locals_:
+        c.start()
+
+    right, left = (s + 1) % n_sp, (s + n_sp - 1) % n_sp
+    halos = []
+    for i, (src, dst) in enumerate(((k_ref, kext), (v_ref, vext))):
+        halos.append((src.at[pl.ds(tok - WINDOW, WINDOW)], dst.at[pl.ds(0, WINDOW)], 2 * i, right))
+        halos.append((src.at[pl.ds(0, WINDOW)], dst.at[pl.ds(tok + WINDOW, WINDOW)], 2 * i + 1, left))
+    halos.append((drow_ref.at[nb - 1], dext.at[0], 4, right))
+    halos.append((drow_ref.at[0], dext.at[nb + 1], 5, left))
+    halo_copies = [rcopy(a, b, halo_s.at[i], halo_r.at[i], to, t) for a, b, i, to in halos]
+    for c in halo_copies:
+        c.start()
+
+    def up_copy(m, slot, sem):
+        return rcopy(piece(m, slot), piece(m, slot), sem, w_r.at[m, slot], s + Y, t)
+
+    def down_copy(m, slot, sem):
+        return rcopy(piece(m, slot), piece(m, slot), sem, w_r.at[m, slot], s - Y, t)
+
+    def z_sem(m, way, zz, yy):
+        return b_s.at[way, zz * Y + yy] if m == 3 else w_s.at[m, way, zz]
+
+    def send_up(m, zz, yy):
+        @pl.when(z + 1 < Z)
+        def _():
+            up_copy(m, zz * Y + yy, z_sem(m, 0, zz, yy)).start()
+
+    def send_down(m, zz, yy):
+        @pl.when(z > 0)
+        def _():
+            down_copy(m, zz * Y + yy, z_sem(m, 1, zz, yy)).start()
+
+    def y_copies(m, zz):
+        slot = zz * Y + y
+        return [
+            rcopy(piece(m, slot), piece(m, slot), w_s.at[m, 1 + j, zz], w_r.at[m, slot], z * Y + (y + j) % Y, t)
+            for j in range(1, Y)
+        ]
+
+    def send_y(m, zz):
+        for c in y_copies(m, zz):
+            c.start()
+
+    def tp_peers():
+        return [(t + j) % T for j in range(1, T)]
+
+    for c in locals_[:1]:
+        c.wait()
+    send_y(3, z)
+    for m in (0, 1):
+        locals_[1 + m].wait()
+        send_up(m, z, y)
+        send_down(m, z, y)
+        send_y(m, z)
+    locals_[3].wait()
+    wo_copies = [rcopy(WO.at[t], WO.at[t], wo_s.at[j], wo_r.at[t], s, p) for j, p in enumerate(tp_peers())]
+    for c in wo_copies:
+        c.start()
+
+    attend(
+        n_sp, s, q_ref, k_ref, v_ref, drow_ref, dcol_ref, sink_ref, kext, vext, dext, att,
+        lambda: [arrived(b, halo_r.at[i]) for a, b, i, to in halos],
+    )
+
     at_copies = [
         rcopy(att.at[pl.ds(pl.multiple_of(p * own, own), own)], rows.at[t], at_s.at[j], at_r.at[t], s, p)
         for j, p in enumerate(tp_peers())
@@ -317,6 +323,291 @@
                     down_copy(m, zz * Y + yy, z_sem(m, 1, zz, yy)).wait_send()
 
 
+def paired_kernel(
+    Z, Y, T, W,
+    q_ref, k_ref, v_ref, drow_ref, dcol_ref, sink_ref, resid_ref, gain_ref, wo_hbm, wg_hbm, wu_hbm, wd_hbm,
+    out_ref,
+    G, U, D, kext, vext, dext, att, rows, WO, mid, NB, gacc, uacc, hid, PT, RT, ZS, ZR,
+    loc_sem, halo_s, halo_r, wo_s, wo_r, at_s, at_r, nb_s, nb_r, pt_s, pt_r, zs_s, zs_r, z_s, y_s, w_r,
+):
+    n_sp = Z * Y
+    s, t = lax.axis_index("sp"), lax.axis_index("tp")
+    z, y, x, core = s // Y, s % Y, t // 2, t % 2
+    par = z % 2
+    s_pair = (z + 1 - 2 * par) * Y + y
+    t_pair = x * 2 + 1 - core
+    tok = q_ref.shape[0]
+    nb = tok // WINDOW
+    own = tok // T
+    all_tok = 2 * tok
+    kb = G.shape[1]
+    half = D.shape[1]
+    offset = wg_hbm.shape[1] - W
+    sent = []
+
+    def rcopy(src, dst, ssem, rsem, sp_to, tp_to):
+        return pltpu.make_async_remote_copy(
+            src_ref=src, dst_ref=dst, send_sem=ssem, recv_sem=rsem,
+            device_id={"sp": sp_to, "tp": tp_to}, device_id_type=MESH,
+        )
+
+    def push(*parts):
+        c = rcopy(*parts)
+        c.start()
+        sent.append(c)
+
+    def arrived(ref, sem):
+        pltpu.make_async_copy(ref, ref, sem).wait()
+
+    def source(m, which):
+        if m < 2:
+            return (wg_hbm, wu_hbm)[m].at[:, pl.ds(pl.multiple_of(which * offset, 128), W)]
+        return wd_hbm.at[pl.ds(pl.multiple_of(which * half, 16), half)]
+
+    def piece(m, slot):
+        return (G, U, D)[m].at[slot]
+
+    def tp_peers():
+        return [(t + j) % T for j in range(1, T)]
+
+    def x_peers():
+        return [((x + j) % (T // 2)) * 2 + core for j in range(1, T // 2)]
+
+    right, left = (s + 1) % n_sp, (s + n_sp - 1) % n_sp
+    halos = []
+    for i, (src, dst) in enumerate(((k_ref, kext), (v_ref, vext))):
+        halos.append((src.at[pl.ds(tok - WINDOW, WINDOW)], dst.at[pl.ds(0, WINDOW)], 2 * i, right))
+        halos.append((src.at[pl.ds(0, WINDOW)], dst.at[pl.ds(tok + WINDOW, WINDOW)], 2 * i + 1, left))
+    halos.append((drow_ref.at[nb - 1], dext.at[0], 4, right))
+    halos.append((drow_ref.at[0], dext.at[nb + 1], 5, left))
+    for a, b, i, to in halos:
+        push(a, b, halo_s.at[i], halo_r.at[i], to, t)
+
+    locals_ = [pltpu.make_async_copy(source(m, par), piece(m, s), loc_sem.at[m]) for m in range(3)]
+    locals_.append(pltpu.make_async_copy(wo_hbm, WO.at[t], loc_sem.at[3]))
+    for c in locals_:
+        c.start()
+
+    def z_copy(m, zz):
+        return rcopy(source(m, zz % 2), piece(m, s), z_s.at[m, zz], w_r.at[m, s], zz * Y + y, t)
+
+    def send_z(m, r):
+        for sign in (-1, 1):
+            zz = z + sign * r
+
+            @pl.when((zz >= 0) & (zz < Z))
+            def _():
+                z_copy(m, zz).start()
+
+    def y_copies(m, zz):
+        slot = zz * Y + y
+        return [
+            rcopy(piece(m, slot), piece(m, slot), y_s.at[m, j, zz], w_r.at[m, slot], z * Y + (y + j) % Y, t)
+            for j in range(1, Y)
+        ]
+
+    def send_y(m, zz):
+        for c in y_copies(m, zz):
+            c.start()
+
+    def handle(ms, r):
+        for m in ms:
+            for sign in (-1, 1):
+                zz = z + sign * r
+
+                @pl.when((zz >= 0) & (zz < Z))
+                def _():
+                    arrived(piece(m, zz * Y + y), w_r.at[m, zz * Y + y])
+                    send_y(m, zz)
+
+    for r in range(1, Z):
+        for m in (0, 1):
+            send_z(m, r)
+    for m in (0, 1):
+        locals_[m].wait()
+        send_y(m, z)
+    locals_[2].wait()
+    locals_[3].wait()
+    for j, p in enumerate(x_peers() + [t_pair]):
+        push(WO.at[t], WO.at[t], wo_s.at[j], wo_r.at[t], s, p)
+
+    attend(
+        Z * Y, s, q_ref, k_ref, v_ref, drow_ref, dcol_ref, sink_ref, kext, vext, dext, att,
+        lambda: [arrived(b, halo_r.at[i]) for a, b, i, to in halos],
+    )
+    for j, p in enumerate(tp_peers()):
+        push(att.at[pl.ds(pl.multiple_of(p * own, own), own)], rows.at[t], at_s.at[j], at_r.at[t], s, p)
+    rows[t] = att[pl.ds(pl.multiple_of(t * own, own), own)]
+
+    handle((0, 1), 1)
+
+    for j, p in enumerate(x_peers()):
+        arrived(WO.at[p], wo_r.at[p])
+        push(WO.at[p], WO.at[p], wo_s.at[T // 2 + j], wo_r.at[p], s, t_pair)
+    for p in [t_pair] + [(p // 2) * 2 + 1 - core for p in x_peers()]:
+        arrived(WO.at[p], wo_r.at[p])
+    for p in tp_peers():
+        arrived(rows.at[p], at_r.at[p])
+    middle = resid_ref[...].astype(jnp.float32)
+    for i in range(T):
+        middle = middle + jnp.dot(rows[i], WO[i], preferred_element_type=jnp.float32)
+    mid[...] = middle
+    normed = (
+        middle * lax.rsqrt(jnp.mean(middle * middle, axis=-1, keepdims=True) + norm_eps) * gain_ref[...]
+    ).astype(jnp.bfloat16)
+
+    def at_rows(p, which):
+        return pl.ds(pl.multiple_of((p * 2 + which) * own, own), own)
+
+    for i in range(n_sp):
+        NB[i, at_rows(t, par)] = normed[:, i * kb:(i + 1) * kb]
+
+    def push_rows(p, which, k, sp_to, tp_to):
+        part = NB.at[:, at_rows(p, which)]
+        push(part, part, nb_s.at[k], nb_r.at[p, which], sp_to, tp_to)
+
+    def wait_rows(p, which):
+        arrived(NB.at[:, at_rows(p, which)], nb_r.at[p, which])
+
+    n_x = T // 2
+    push_rows(t, par, 0, s_pair, t)
+    for j, p in enumerate(x_peers() + [t_pair]):
+        push_rows(t, par, 1 + j, s, p)
+    for r in range(1, Z):
+        send_z(2, r)
+    for r in range(2, max(3, Z - 1)):
+        if r < Z:
+            handle((0, 1), r)
+    wait_rows(t, 1 - par)
+    for j, p in enumerate(x_peers() + [t_pair]):
+        push_rows(t, 1 - par, 1 + n_x + j, s, p)
+    for r in range(max(3, Z - 1), Z):
+        handle((0, 1), r)
+    send_y(2, z)
+    for j, p in enumerate(x_peers()):
+        for i, which in enumerate((par, 1 - par)):
+            wait_rows(p, which)
+            push_rows(p, which, 1 + 2 * n_x + 2 * j + i, s, t_pair)
+    for p in [t_pair] + [(p // 2) * 2 + 1 - core for p in x_peers()]:
+        for which in (par, 1 - par):
+            wait_rows(p, which)
+
+    step = min(all_tok, 256)
+
+    def each(r, body):
+        @pl.loop(0, (2 if r else 1) * Y)
+        def _(i):
+            joff = i % Y
+            zz = z + (2 * (i // Y) - 1) * r
+            slot = zz * Y + (y + joff) % Y
+
+            @pl.when((zz >= 0) & (zz < Z))
+            def _():
+                body(slot, joff)
+
+    def gate_up(r):
+        def body(slot, joff):
+            @pl.when(joff > 0)
+            def _():
+                for m in (0, 1):
+                    arrived(piece(m, slot), w_r.at[m, slot])
+
+            @pl.loop(0, all_tok // step)
+            def _(i):
+                at = pl.ds(pl.multiple_of(i * step, step), step)
+                rows_in = NB[slot, at]
+                gacc[at] += jnp.dot(rows_in, G[slot], preferred_element_type=jnp.float32)
+                uacc[at] += jnp.dot(rows_in, U[slot], preferred_element_type=jnp.float32)
+
+        each(r, body)
+
+    def peer_rows(p):
+        return pl.ds(pl.multiple_of(p * 2 * own, 2 * own), 2 * own)
+
+    def down(r):
+        def body(slot, joff):
+            @pl.when(joff > 0)
+            def _():
+                arrived(piece(2, slot), w_r.at[2, slot])
+
+            @pl.loop(0, all_tok // step)
+            def _(i):
+                at = pl.ds(pl.multiple_of(i * step, step), step)
+                PT[slot, at] = jnp.dot(hid[at], D[slot], preferred_element_type=jnp.float32).astype(jnp.bfloat16)
+
+            for j, p in enumerate(tp_peers()):
+                rcopy(PT.at[slot, peer_rows(p)], RT.at[t, slot], pt_s.at[j], pt_r.at[t, slot], s, p).start()
+
+        each(r, body)
+
+    def reduce(r):
+        def body(slot, joff):
+            for p in tp_peers():
+                arrived(RT.at[p, slot], pt_r.at[p, slot])
+            here = pl.ds(pl.multiple_of(par * own, own), own)
+            there = pl.ds(pl.multiple_of((1 - par) * own, own), own)
+            away = PT[slot, at_rows(t, 1 - par)].astype(jnp.float32)
+            for p in tp_peers():
+                away = away + RT[p, slot, there].astype(jnp.float32)
+            ZS[slot] = away.astype(jnp.bfloat16)
+            rcopy(ZS.at[slot], ZR.at[slot], zs_s, zs_r, s_pair, t).start()
+
+        each(r, body)
+
+    gacc[...] = jnp.zeros_like(gacc)
+    uacc[...] = jnp.zeros_like(uacc)
+    gate_up(0)
+    gate_up(1)
+    handle((2,), 1)
+    for r in range(2, Z):
+        gate_up(r)
+
+    @pl.loop(0, all_tok // WINDOW)
+    def _(i):
+        at = pl.ds(pl.multiple_of(i * WINDOW, WINDOW), WINDOW)
+        gate = gacc[at]
+        act = (gate / (1.0 + jnp.exp(-gate)) * uacc[at]).astype(jnp.bfloat16)
+
+        @pl.when(par == 0)
+        def _():
+            hid[at] = act[:, :half]
+
+        @pl.when(par == 1)
+        def _():
+            hid[at] = act[:, W - half:]
+
+    down(0)
+    for r in range(1, Z):
+        if r + 1 < Z:
+            handle((2,), r + 1)
+        down(r)
+        reduce(r - 1)
+    reduce(Z - 1)
+
+    arrived(ZR, zs_r)
+    here = pl.ds(pl.multiple_of(par * own, own), own)
+    for i in range(n_sp):
+        cols = slice(i * kb, (i + 1) * kb)
+        total = mid[:, cols] + PT[i, at_rows(t, par)].astype(jnp.float32) + ZR[i].astype(jnp.float32)
+        for p in tp_peers():
+            total = total + RT[p, i, here].astype(jnp.float32)
+        out_ref[:, cols] = total.astype(jnp.bfloat16)
+
+    for c in sent:
+        c.wait_send()
+    for j, p in enumerate(tp_peers()):
+        arrived(PT.at[:, peer_rows(p)], pt_s.at[j])
+    arrived(ZS, zs_s)
+    for m in range(3):
+        for zz in range(Z):
+            for c in y_copies(m, zz):
+                c.wait_send()
+
+            @pl.when(z != zz)
+            def _():
+                z_copy(m, zz).wait_send()
+
+
 def shards(Z, Y, T, q, k, v, doc_ids, sinks, resid, w_out, gain, wg, wu, wd):
     n_sp = Z * Y
     tok, (kb, ff), d = q.shape[0], wg.shape, resid.shape[1]
@@ -327,10 +618,37 @@
     vmem, hbm = pl.BlockSpec(memory_space=pltpu.VMEM), pl.BlockSpec(memory_space=pl.ANY)
     dma = pltpu.SemaphoreType.DMA
     V = pltpu.VMEM
+    specs = [vmem] * 5 + [pl.BlockSpec(memory_space=pltpu.SMEM)] + [vmem] * 2 + [hbm] * 4
+    params = pltpu.CompilerParams(has_side_effects=True, vmem_limit_bytes=60 * 1024 * 1024)
+    operands = (q, k, v, drow, dcol, sinks, resid, gain.reshape(1, d), w_out, wg, wu, wd)
+    half = ff // 2
+    W = -(-half // 128) * 128
+    if Z % 2 == 0 and T % 2 == 0 and (ff - W) % 128 == 0 and half % 16 == 0 and kb % 128 == 0:
+        return pl.pallas_call(
+            functools.partial(paired_kernel, Z, Y, T, W),
+            out_shape=jax.ShapeDtypeStruct((own, d), bf),
+            in_specs=specs,
+            out_specs=vmem,
+            scratch_shapes=[
+                V((n_sp, kb, W), bf), V((n_sp, kb, W), bf), V((n_sp, half, wd.shape[1]), bf),
+                V((tok + 2 * WINDOW, k.shape[1]), bf), V((tok + 2 * WINDOW, k.shape[1]), bf),
+                V((nb + 2, 8, WINDOW), jnp.int32),
+                V((tok, q.shape[1]), bf), V((T, own, q.shape[1]), bf), V((T,) + w_out.shape, bf),
+                V((own, d), f32), V((n_sp, 2 * tok, kb), bf),
+                V((2 * tok, W), f32), V((2 * tok, W), f32), V((2 * tok, half), bf),
+                V((n_sp, 2 * tok, kb), bf), V((T, n_sp, 2 * own, kb), bf),
+                V((n_sp, own, kb), bf), V((n_sp, own, kb), bf),
+                dma((4,)), dma((6,)), dma((6,)),
+                dma((T,)), dma((T,)), dma((T,)), dma((T,)), dma((2 * T + 1,)), dma((T, 2)),
+                dma((T,)), dma((T, n_sp)), dma(()), dma(()),
+                dma((3, Z)), dma((3, Y, Z)), dma((3, n_sp)),
+            ],
+            compiler_params=params,
+        )(*operands)
     return pl.pallas_call(
         functools.partial(kernel, Z, Y, T),
         out_shape=jax.ShapeDtypeStruct((own, d), bf),
-        in_specs=[vmem] * 5 + [pl.BlockSpec(memory_space=pltpu.SMEM)] + [vmem] * 2 + [hbm] * 4,
+        in_specs=specs,
         out_specs=vmem,
         scratch_shapes=[
             V((n_sp, kb, ff), bf), V((n_sp, kb, ff), bf), V((n_sp, ff, wd.shape[1]), bf),
@@ -343,8 +661,8 @@
             dma((T,)), dma((T,)), dma((T,)), dma((T,)), dma((T,)), dma((T,)), dma((T,)), dma((T,)),
             dma((4, 1 + Y, Z)), dma((4, n_sp)), dma((2, n_sp)),
         ],
-        compiler_params=pltpu.CompilerParams(has_side_effects=True, vmem_limit_bytes=60 * 1024 * 1024),
-    )(q, k, v, drow, dcol, sinks, resid, gain.reshape(1, d), w_out, wg, wu, wd)
+        compiler_params=params,
+    )(*operands)
 
 
 def solution(mesh):

time: 215 us -> 184 us (0.86)
  the two profiles are of different devices: /device:TPU:0 before, /device:TPU:21 now
where the time goes in v2:
time: 184 us
  Pallas kernels  180 us (98%)
  local copies, waits for them, and re-layouts  4 us (2%)
    pallas_call x1, Pallas kernels, shards(): pl.pallas_call(functools.partial(paired_kernel, Z, Y, T, W), out_shape=ja...  180 us

profile of v2, /device:TPU:21, one launch (start us, length us, event | category | flops | bytes accessed | tf_op | source)
XLA Modules:
  0.0 183.6 jit_solution(3066701535337010692)
XLA Ops:
  0.0 0.0 copy-start
  0.0 0.7 copy-done
  0.7 0.6 broadcast_in_dim.14.drow_ref
  1.3 0.8 broadcast_in_dim.15.dcol_ref
  2.1 179.6 %shard_map.109 = bf16[128,2048]{1,0:T(8,128)(2,1)} custom-call(bf16[512,256]{1,0:T(8,128)(2,1)} %q_ref.1, bf16[512,128]{1,0:T(8,128)(2,1)} %k_ref.1, bf16[512,128]{1,0:T(8,128)(2,1)} %v_ref.1, s32[4,8,128]{2,1,0:T(8,128)} %broadcast_in_dim.14.drow_ref, s32[512,128]{1,0:T(8,128)} %broadcast_in_dim.15.dcol_ref, f32[4]{0:T(128)} %sink_ref.1, ...), custom_call_target="tpu_custom_call" | custom-call | tf_op jit(solution)/shard_map/pallas_call | solution.py:627
  181.7 1.9 %copy.13 = bf16[128,2048]{1,0:T(8,128)(2,1)} copy(bf16[128,2048]{1,0:T(8,128)(2,1)} %shard_map.109) | data formatting | bytes 1048576
Async XLA Ops:
  0.0 0.7 copy-start

commit v3 on v2

--- a/solution.py
+++ b/solution.py
@@ -327,8 +327,8 @@
     Z, Y, T, W,
     q_ref, k_ref, v_ref, drow_ref, dcol_ref, sink_ref, resid_ref, gain_ref, wo_hbm, wg_hbm, wu_hbm, wd_hbm,
     out_ref,
-    G, U, D, kext, vext, dext, att, rows, WO, mid, NB, gacc, uacc, hid, PT, RT, ZS, ZR,
-    loc_sem, halo_s, halo_r, wo_s, wo_r, at_s, at_r, nb_s, nb_r, pt_s, pt_r, zs_s, zs_r, z_s, y_s, w_r,
+    G, U, D, kext, vext, dext, att, rows, WO, mid, NB, gacc, uacc, hid, PT, RD, XS, RT, ZS, ZR,
+    loc_sem, halo_s, halo_r, wo_s, wo_r, at_s, at_r, nb_s, nb_r, pt_s, pt_r, xs_s, xs_r, zs_s, zs_r, z_s, y_s, w_r,
 ):
     n_sp = Z * Y
     s, t = lax.axis_index("sp"), lax.axis_index("tp")
@@ -420,7 +420,7 @@
                     arrived(piece(m, zz * Y + y), w_r.at[m, zz * Y + y])
                     send_y(m, zz)
 
-    for r in range(1, Z):
+    for r in range(1, max(2, Z - 1)):
         for m in (0, 1):
             send_z(m, r)
     for m in (0, 1):
@@ -473,6 +473,9 @@
     push_rows(t, par, 0, s_pair, t)
     for j, p in enumerate(x_peers() + [t_pair]):
         push_rows(t, par, 1 + j, s, p)
+    for r in range(max(2, Z - 1), Z):
+        for m in (0, 1):
+            send_z(m, r)
     for r in range(1, Z):
         send_z(2, r)
     for r in range(2, max(3, Z - 1)):
@@ -535,20 +538,30 @@
                 at = pl.ds(pl.multiple_of(i * step, step), step)
                 PT[slot, at] = jnp.dot(hid[at], D[slot], preferred_element_type=jnp.float32).astype(jnp.bfloat16)
 
-            for j, p in enumerate(tp_peers()):
-                rcopy(PT.at[slot, peer_rows(p)], RT.at[t, slot], pt_s.at[j], pt_r.at[t, slot], s, p).start()
+            for i in range(n_x):
+                rows_out = PT.at[slot, peer_rows(i * 2 + 1 - core)]
+                rcopy(rows_out, RD.at[slot, i], pt_s.at[i], pt_r.at[slot], s, t_pair).start()
+
+        each(r, body)
+
+    def mix(r):
+        def body(slot, joff):
+            arrived(RD.at[slot], pt_r.at[slot])
+            for j, p in enumerate(x_peers()):
+                both = PT[slot, peer_rows(p)].astype(jnp.float32) + RD[slot, p // 2].astype(jnp.float32)
+                XS[slot, j] = both.astype(jnp.bfloat16)
+                rcopy(XS.at[slot, j], RT.at[x, slot], xs_s.at[j], xs_r.at[x, slot], s, p).start()
 
         each(r, body)
 
     def reduce(r):
         def body(slot, joff):
-            for p in tp_peers():
-                arrived(RT.at[p, slot], pt_r.at[p, slot])
-            here = pl.ds(pl.multiple_of(par * own, own), own)
+            for p in x_peers():
+                arrived(RT.at[p // 2, slot], xs_r.at[p // 2, slot])
             there = pl.ds(pl.multiple_of((1 - par) * own, own), own)
-            away = PT[slot, at_rows(t, 1 - par)].astype(jnp.float32)
-            for p in tp_peers():
-                away = away + RT[p, slot, there].astype(jnp.float32)
+            away = PT[slot, at_rows(t, 1 - par)].astype(jnp.float32) + RD[slot, x, there].astype(jnp.float32)
+            for p in x_peers():
+                away = away + RT[p // 2, slot, there].astype(jnp.float32)
             ZS[slot] = away.astype(jnp.bfloat16)
             rcopy(ZS.at[slot], ZR.at[slot], zs_s, zs_r, s_pair, t).start()
 
@@ -581,22 +594,29 @@
         if r + 1 < Z:
             handle((2,), r + 1)
         down(r)
-        reduce(r - 1)
-    reduce(Z - 1)
+        mix(r - 1)
+        if r > 1:
+            reduce(r - 2)
+    mix(Z - 1)
+    for r in range(max(0, Z - 2), Z):
+        reduce(r)
 
     arrived(ZR, zs_r)
     here = pl.ds(pl.multiple_of(par * own, own), own)
     for i in range(n_sp):
         cols = slice(i * kb, (i + 1) * kb)
         total = mid[:, cols] + PT[i, at_rows(t, par)].astype(jnp.float32) + ZR[i].astype(jnp.float32)
-        for p in tp_peers():
-            total = total + RT[p, i, here].astype(jnp.float32)
+        total = total + RD[i, x, here].astype(jnp.float32)
+        for p in x_peers():
+            total = total + RT[p // 2, i, here].astype(jnp.float32)
         out_ref[:, cols] = total.astype(jnp.bfloat16)
 
     for c in sent:
         c.wait_send()
-    for j, p in enumerate(tp_peers()):
-        arrived(PT.at[:, peer_rows(p)], pt_s.at[j])
+    for i in range(n_x):
+        arrived(PT.at[:, peer_rows(i * 2 + 1 - core)], pt_s.at[i])
+    for j in range(n_x - 1):
+        arrived(XS.at[:, j], xs_s.at[j])
     arrived(ZS, zs_s)
     for m in range(3):
         for zz in range(Z):
@@ -636,11 +656,12 @@
                 V((tok, q.shape[1]), bf), V((T, own, q.shape[1]), bf), V((T,) + w_out.shape, bf),
                 V((own, d), f32), V((n_sp, 2 * tok, kb), bf),
                 V((2 * tok, W), f32), V((2 * tok, W), f32), V((2 * tok, half), bf),
-                V((n_sp, 2 * tok, kb), bf), V((T, n_sp, 2 * own, kb), bf),
+                V((n_sp, 2 * tok, kb), bf), V((n_sp, T // 2, 2 * own, kb), bf),
+                V((n_sp, max(1, T // 2 - 1), 2 * own, kb), bf), V((T // 2, n_sp, 2 * own, kb), bf),
                 V((n_sp, own, kb), bf), V((n_sp, own, kb), bf),
                 dma((4,)), dma((6,)), dma((6,)),
                 dma((T,)), dma((T,)), dma((T,)), dma((T,)), dma((2 * T + 1,)), dma((T, 2)),
-                dma((T,)), dma((T, n_sp)), dma(()), dma(()),
+                dma((T,)), dma((n_sp,)), dma((T,)), dma((T, n_sp)), dma(()), dma(()),
                 dma((3, Z)), dma((3, Y, Z)), dma((3, n_sp)),
             ],
             compiler_params=params,

time: 184 us -> 172 us (0.935)
  the two profiles are of different devices: /device:TPU:21 before, /device:TPU:16 now
where the time goes in v3:
time: 172 us
  Pallas kernels  168 us (98%)
  local copies, waits for them, and re-layouts  4 us (2%)
    pallas_call x1, Pallas kernels, shards(): pl.pallas_call(functools.partial(paired_kernel, Z, Y, T, W), out_shape=ja...  168 us

profile of v3, /device:TPU:16, one launch (start us, length us, event | category | flops | bytes accessed | tf_op | source)
XLA Modules:
  0.0 171.7 jit_solution(8702977589222237064)
XLA Ops:
  0.0 0.0 copy-start
  0.0 0.7 copy-done
  0.7 0.6 broadcast_in_dim.14.drow_ref
  1.3 0.8 broadcast_in_dim.15.dcol_ref
  2.1 167.7 %shard_map.109 = bf16[128,2048]{1,0:T(8,128)(2,1)} custom-call(bf16[512,256]{1,0:T(8,128)(2,1)} %q_ref.1, bf16[512,128]{1,0:T(8,128)(2,1)} %k_ref.1, bf16[512,128]{1,0:T(8,128)(2,1)} %v_ref.1, s32[4,8,128]{2,1,0:T(8,128)} %broadcast_in_dim.14.drow_ref, s32[512,128]{1,0:T(8,128)} %broadcast_in_dim.15.dcol_ref, f32[4]{0:T(128)} %sink_ref.1, ...), custom_call_target="tpu_custom_call" | custom-call | tf_op jit(solution)/shard_map/pallas_call | solution.py:647
  169.8 1.9 %copy.13 = bf16[128,2048]{1,0:T(8,128)(2,1)} copy(bf16[128,2048]{1,0:T(8,128)(2,1)} %shard_map.109) | data formatting | bytes 1048576
Async XLA Ops:
  0.0 0.7 copy-start
